TPU v7x, 32 devices: a whole 2x2x4 slice. The times are simulated.
32 devices in a mesh: fs: 8 (over z, y), tp: 4 (over x, core).
Axes of the slice: x: 2, y: 2, z: 4, core: 2. Of those that a mesh axis runs over, the one named last changes fastest.
Arguments:
- tokens: bfloat16 [3072, 2048], P('tp'), may hold values from -6 to 6
- norm_gain: float32 [2048], P('fs'), may hold values from 0.1 to 1.9
- gate_weight: float32 [4, 2048, 8192], P(None, 'fs', 'tp'), may hold values from -0.125 to 0.125
- up_weight: float32 [4, 2048, 8192], P(None, 'fs', 'tp'), may hold values from -0.125 to 0.125
- down_weight: float32 [4, 8192, 2048], P(None, 'fs', 'tp'), may hold values from -0.0625 to 0.0625
- routes: int32 [3072, 2], P('tp'), may hold values from 0 to 3, all different within a row; in each aligned block of 768 rows (0 to 767, 768 to 1535, ...) at most 480 rows name the same one
- route_logit: float32 [3072, 2], P('tp'), may hold values from -6 to 6
Outputs:
- gate_out: bfloat16 [4, 2048, 8192], P(None, None, 'fs')
- up_out: bfloat16 [4, 2048, 8192], P(None, None, 'fs')
- down_out: bfloat16 [4, 8192, 2048], P(None, 'fs')
- mixed: bfloat16 [3072, 2048], P(('tp', 'fs'))
Inputs may be any that keep to these rules, and one draw needn't show every extreme that they name: `routes`: the two experts of a token differ. In each aligned block of 768 tokens (the tokens of one request group) every expert is named by at most 480 tokens, a bound that some block reaches.
All inputs are finite; a program needn't handle non-finite values.
Results may differ from a plain program's by a relative error of at most 0.0082.
Values may be sent and summed in bfloat16 or wider, within the bound.
A program may use at most 192 MiB of HBM per device.

v0:
```python
import functools

import jax
import jax.numpy as jnp
from jax import lax
from jax.experimental import pallas as pl
from jax.experimental.pallas import tpu as pltpu
from jax.sharding import PartitionSpec as P

EPS = 0.5
MESH = pl.DeviceIdType.MESH
VMEM_LIMIT = 62 * 1024 * 1024


def spread(
    gain, gate_f32, up_f32, down_f32,
    gate_all, up_all, down_all, gate_far, up_far,
    own, down, stage, down_stage, load,
    across_send, across_recv, near_send, near_recv, far_send, twin_send, twin_recv, onward_send,
    down_send, down_recv,
):
    _, experts, depth, width = own.shape
    features, units = gate_all.shape[1:]
    per = width // units
    fs, tp = lax.axis_index("fs"), lax.axis_index("tp")
    half, side = tp // 2, tp % 2
    twin = half * 2 + 1 - side
    across = (1 - half) * 2 + side
    col = down.shape[2]
    group = fs // per
    apart = group // 2 != half
    close = group // 2 == half
    far, full = (gate_far, up_far), (gate_all, up_all)

    def remote(src, dst, send, recv, fs_to, tp_to):
        return pltpu.make_async_remote_copy(
            src_ref=src, dst_ref=dst, send_sem=send, recv_sem=recv,
            device_id=(fs_to, tp_to), device_id_type=MESH,
        )

    def columns(owner):
        return pl.ds(pl.multiple_of(owner * col, col), col)

    def only(condition, needed, action):
        if needed:
            pl.when(condition)(action)
        else:
            action()

    pieces = [(a, e) for e in range(experts) for a in range(2)]
    early, late, rest = pieces[:1], pieces[1:3], pieces[3:]
    rows = pl.ds(pl.multiple_of(fs * depth, depth), depth)

    def crossing(a, e):
        return remote(
            own.at[a, e], far[a].at[e], across_send.at[a, e], across_recv.at[a, e], fs, across
        )

    def deal(source, a, e, owner, sem):
        for h in range(per):
            remote(
                source.at[:, pl.ds(h * units, units)],
                full[a].at[e, rows, :],
                sem.at[a, e],
                near_recv.at[a, e],
                owner * per + h,
                twin,
            ).start()

    def fetch(n):
        a, e = pieces[n]
        return pltpu.make_async_copy((gate_f32, up_f32)[a].at[e], stage.at[n % 2], load.at[n % 2])

    tile = min(depth, 32)
    fetch(0).start()
    for n, piece in enumerate(pieces):
        a, e = piece
        if n + 1 < len(pieces):
            fetch(n + 1).start()
        fetch(n).wait()

        def scale(i, carry, a=a, e=e, n=n):
            at = pl.ds(pl.multiple_of(i * tile, tile), tile)
            own[a, e, at, :] = (stage[n % 2, at, :] * gain[at, :]).astype(own.dtype)
            return carry

        lax.fori_loop(0, depth // tile, scale, 0)
        only(close, piece in late, lambda: crossing(a, e).start())
        only(close, piece in early, lambda: deal(own.at[a, e], a, e, tp, near_send))

    def fetch_down(e):
        return pltpu.make_async_copy(down_f32.at[e], down_stage.at[e % 2], load.at[2 + e % 2])

    fetch_down(0).start()
    for e in range(experts):
        if e + 1 < experts:
            fetch_down(e + 1).start()
        fetch_down(e).wait()
        short = min(units, 128)

        def narrow(i, carry, e=e):
            at = pl.ds(pl.multiple_of(i * short, short), short)
            down[e, at, :] = down_stage[e % 2, at, :].astype(down.dtype)
            return carry

        lax.fori_loop(0, units // short, narrow, 0)

    down_near = remote(
        down, down_all.at[:, :, columns(tp)], down_send.at[0], down_recv.at[0], fs, twin
    )
    down_near.start()
    down_far = remote(
        down, down_all.at[:, :, columns(tp)], down_send.at[1], down_recv.at[1], fs, across
    )
    down_far.start()

    for piece in pieces:
        a, e = piece

        def relay(a=a, e=e):
            crossing(a, e).wait_recv()
            deal(far[a].at[e], a, e, across, far_send)

        only(apart, piece in late, relay)

    def hand_down(owner, index):
        return remote(
            down_all.at[:, :, columns(owner)], down_all.at[:, :, columns(owner)],
            down_send.at[index], down_recv.at[index], fs, twin,
        )

    lands = side == 1 - group % 2
    away = pl.ds(pl.multiple_of((1 - group // 2) * (features // 2), features // 2), features // 2)

    def hand(a, e):
        return remote(
            full[a].at[e], full[a].at[e], twin_send.at[a, e], twin_recv.at[a, e], fs, twin
        )

    def onward(a, e):
        part = full[a].at[e, away, :]
        return remote(part, part, onward_send.at[a, e], near_recv.at[a, e], fs, across)

    def block_done(a, e, sem):
        pltpu.make_async_copy(full[a].at[e], full[a].at[e], sem.at[a, e]).wait()

    def take(group_of, forward):
        for a, e in group_of:
            block_done(a, e, near_recv)
            if forward:
                onward(a, e).start()
            hand(a, e).start()

    @pl.when(lands)
    def _():
        pl.when(close)(lambda: take(late, True))
        pl.when(apart)(lambda: take(early, True))

    down_near.wait_recv()
    echo = hand_down(twin, 2)
    echo.start()
    down_far.wait_recv()
    passed = hand_down(across, 3)
    passed.start()

    @pl.when(lands)
    def _():
        take(rest, False)
        pl.when(close)(lambda: take(early, False))
        pl.when(apart)(lambda: take(late, False))
        for a, e in pieces:
            hand(a, e).wait_send()

        def sent(group_of):
            for a, e in group_of:
                onward(a, e).wait_send()

        pl.when(close)(lambda: sent(late))
        pl.when(apart)(lambda: sent(early))

    @pl.when(jnp.logical_not(lands))
    def _():
        for a, e in pieces:
            hand(a, e).wait_recv()

    for piece in pieces:
        a, e = piece

        def dealt(sem, a=a, e=e):
            pltpu.make_async_copy(far[a].at[e], far[a].at[e], sem.at[a, e]).wait()

        only(close, piece in late, lambda: crossing(a, e).wait_send())
        only(close, piece in early, lambda: dealt(near_send))
        only(apart, piece in late, lambda: dealt(far_send))
    down_near.wait_send()
    down_far.wait_send()
    echo.wait()
    passed.wait()


def apply_experts(x, weight, gate, up, down, gate_out, up_out, down_out, part, total):
    expert, block = pl.program_id(0), pl.program_id(1)
    gate_out[...] = gate[...]
    up_out[...] = up[...]
    down_out[...] = down[...]
    rows = x.shape[0]
    tile = rows // 2

    @pl.when(jnp.logical_and(expert == 0, block == 0))
    def _():
        total[...] = jnp.zeros_like(total)

    def step(i, carry):
        at = pl.ds(pl.multiple_of(i * tile, tile), tile)
        mine = x[at, :]
        gate_val = jnp.dot(mine, gate[0], preferred_element_type=jnp.float32)
        up_val = jnp.dot(mine, up[0], preferred_element_type=jnp.float32)
        hidden = (jax.nn.silu(gate_val) * up_val).astype(jnp.bfloat16)
        result = jnp.dot(hidden, down[0], preferred_element_type=jnp.float32)
        shares = weight[at, :]
        lane = lax.broadcasted_iota(jnp.int32, shares.shape, 1)
        share = jnp.sum(jnp.where(lane == expert, shares, 0.0), axis=1, keepdims=True)
        total[at, :] += share * result
        return carry

    lax.fori_loop(0, rows // tile, step, 0)

    @pl.when(
        jnp.logical_and(expert == pl.num_programs(0) - 1, block == pl.num_programs(1) - 1)
    )
    def _():
        part[...] = total[...].astype(part.dtype)


def fold(chunks, part, out, low_in, mid, high_in, low_send, low_recv, high_send, high_recv):
    highs, _, rows, width = part.shape
    step = width // chunks
    fs, tp = lax.axis_index("fs"), lax.axis_index("tp")
    high, low = fs // 2, fs % 2
    first = []
    for k in range(chunks):
        copy = pltpu.make_async_remote_copy(
            src_ref=part.at[:, 1 - low, :, pl.ds(k * step, step)],
            dst_ref=low_in.at[k],
            send_sem=low_send.at[k],
            recv_sem=low_recv.at[k],
            device_id=(high * 2 + 1 - low, tp),
            device_id_type=MESH,
        )
        copy.start()
        first.append(copy)
    second = []
    for k in range(chunks):
        first[k].wait_recv()
        mid[k] = (
            part[:, low, :, pl.ds(k * step, step)].astype(jnp.float32)
            + low_in[k].astype(jnp.float32)
        ).astype(mid.dtype)
        for shift in range(1, highs):
            to = lax.rem(high + shift, highs)
            copy = pltpu.make_async_remote_copy(
                src_ref=mid.at[k, to],
                dst_ref=high_in.at[k, shift],
                send_sem=high_send.at[k, shift],
                recv_sem=high_recv.at[k, shift],
                device_id=(to * 2 + low, tp),
                device_id_type=MESH,
            )
            copy.start()
            second.append((k, copy))
    for k in range(chunks):
        total = part[high, low, :, pl.ds(k * step, step)].astype(jnp.float32) + low_in[
            k, high
        ].astype(jnp.float32)
        shift = 0
        for at, copy in second:
            if at == k:
                shift += 1
                copy.wait_recv()
                total = total + high_in[k, shift].astype(jnp.float32)
        out[:, pl.ds(k * step, step)] = total.astype(out.dtype)
    for copy in first:
        copy.wait_send()
    for _, copy in second:
        copy.wait_send()


def shards(fs_size, tokens, norm_gain, gate_weight, up_weight, down_weight, routes, route_logit):
    experts, depth, width = gate_weight.shape
    _, units, col = down_weight.shape
    rows, features = tokens.shape
    floats = tokens.astype(jnp.float32)
    normed = (floats * lax.rsqrt(jnp.mean(floats * floats, axis=1, keepdims=True) + EPS)).astype(
        jnp.bfloat16
    )
    first_share = jax.nn.sigmoid(route_logit[:, 0] - route_logit[:, 1])
    shares = jnp.stack([first_share, 1.0 - first_share], axis=1)
    named = routes[:, :, None] == jnp.arange(experts, dtype=jnp.int32)[None, None, :]
    weight = jnp.sum(jnp.where(named, shares[:, :, None], 0.0), axis=1)

    half = jnp.bfloat16
    anywhere = pl.BlockSpec(memory_space=pl.ANY)
    dma = pltpu.SemaphoreType.DMA
    gate_shape = jax.ShapeDtypeStruct((experts, features, units), half)
    down_shape = jax.ShapeDtypeStruct((experts, units, features), half)
    far_shape = jax.ShapeDtypeStruct((experts, depth, width), half)
    gate_all, up_all, down_all, _, _ = pl.pallas_call(
        spread,
        out_shape=(gate_shape, gate_shape, down_shape, far_shape, far_shape),
        in_specs=[pl.BlockSpec(memory_space=pltpu.VMEM)] + [anywhere] * 3,
        out_specs=(anywhere,) * 5,
        scratch_shapes=[
            pltpu.VMEM((2, experts, depth, width), half),
            pltpu.VMEM((experts, units, col), half),
            pltpu.VMEM((2, depth, width), jnp.float32),
            pltpu.VMEM((2, units, col), jnp.float32),
            dma((4,)),
        ]
        + [dma((2, experts))] * 8
        + [dma((4,))] * 2,
        compiler_params=pltpu.CompilerParams(
            has_side_effects=True, vmem_limit_bytes=VMEM_LIMIT
        ),
        name="spread",
    )(norm_gain[:, None], gate_weight, up_weight, down_weight)

    block = min(units, 512)
    in_wide = pl.BlockSpec((1, features, block), lambda e, j: (e, 0, j))
    in_tall = pl.BlockSpec((1, block, features), lambda e, j: (e, j, 0))
    whole = pl.BlockSpec((rows, features), lambda e, j: (0, 0))
    gate_out, up_out, down_out, part = pl.pallas_call(
        apply_experts,
        grid=(experts, units // block),
        out_shape=(
            gate_shape, gate_shape, down_shape, jax.ShapeDtypeStruct((rows, features), half),
        ),
        in_specs=[
            whole, pl.BlockSpec((rows, experts), lambda e, j: (0, 0)), in_wide, in_wide, in_tall,
        ],
        out_specs=(in_wide, in_wide, in_tall, whole),
        scratch_shapes=[pltpu.VMEM((rows, features), jnp.float32)],
        compiler_params=pltpu.CompilerParams(
            vmem_limit_bytes=VMEM_LIMIT, dimension_semantics=("arbitrary", "arbitrary")
        ),
        name="apply_experts",
    )(normed, weight, gate_all, up_all, down_all)

    highs, mine, chunks = fs_size // 2, rows // fs_size, 4
    step = features // chunks
    vmem = pl.BlockSpec(memory_space=pltpu.VMEM)
    mixed = pl.pallas_call(
        functools.partial(fold, chunks),
        out_shape=jax.ShapeDtypeStruct((mine, features), half),
        in_specs=[vmem],
        out_specs=vmem,
        scratch_shapes=[pltpu.VMEM((chunks, highs, mine, step), half)] * 3
        + [dma((chunks,))] * 2
        + [dma((chunks, highs))] * 2,
        compiler_params=pltpu.CompilerParams(
            has_side_effects=True, vmem_limit_bytes=VMEM_LIMIT // 2
        ),
        name="fold",
    )(part.reshape(highs, 2, mine, features))
    return (gate_out, up_out, down_out, mixed)


def solution(mesh):
    return jax.shard_map(
        functools.partial(shards, mesh.shape["fs"]),
        mesh=mesh,
        in_specs=(
            P("tp", None),
            P("fs"),
            P(None, "fs", "tp"),
            P(None, "fs", "tp"),
            P(None, "fs", "tp"),
            P("tp", None),
            P("tp", None),
        ),
        out_specs=(
            P(None, None, "fs"),
            P(None, None, "fs"),
            P(None, "fs", None),
            P(("tp", "fs"), None),
        ),
        check_vma=False,
    )
```

profile of v0, /device:TPU:0, one launch (start us, length us, event | category | flops | bytes accessed | tf_op | source)
XLA Modules:
  0.0 462.7 jit_solution(6164678039465264335)
XLA Ops:
  0.6 2.6 fusion
  3.2 0.8 broadcast_subtract_fusion
  4.0 0.7 select_reduce_fusion
  4.7 1.5 copy.16.gain
  6.2 0.9 copy.17.weight
  7.2 4.1 fusion.1.x
  11.3 333.6 %spread.1 = (bf16[4,2048,1024]{2,1,0:T(8,128)(2,1)}, bf16[4,2048,1024]{2,1,0:T(8,128)(2,1)}, bf16[4,1024,2048]{2,1,0:T(8,128)(2,1)}, bf16[4,256,2048]{2,1,0:T(8,128)(2,1)}, bf16[4,256,2048]{2,1,0:T(8,128)(2,1)}) custom-call(f32[256,1]{1,0:T(8,128)} %copy.16.gain, f32[4,256,2048]{2,1,0:T(8,128)} %gate_f32.1, f32[4,256,2048]{2,1,0:T(8,128)} %up_f32.1, ...), custom_call_target="tpu_custom_call" | custom-call | tf_op jit(solution)/shard_map/spread/pallas_call | solution.py:307
  344.9 54.9 %apply_experts.1 = (bf16[4,2048,1024]{2,1,0:T(8,128)(2,1)}, bf16[4,2048,1024]{2,1,0:T(8,128)(2,1)}, bf16[4,1024,2048]{2,1,0:T(8,128)(2,1)}, bf16[768,2048]{1,0:T(8,128)(2,1)}) custom-call(bf16[768,2048]{1,0:T(8,128)(2,1)} %fusion.1.x, f32[768,4]{1,0:T(8,128)} %copy.17.weight, bf16[4,2048,1024]{2,1,0:T(8,128)(2,1)} %get-tuple-element.11.gate, ...), custom_call_target="tpu_custom_call" | custom-call | tf_op jit(solution)/shard_map/apply_experts/pallas_call | solution.py:331
  399.8 0.0 copy-start
  399.8 1.9 copy-done
  401.7 60.3 %fold.1 = bf16[96,2048]{1,0:T(8,128)(2,1)S(1)} custom-call(bf16[4,2,96,2048]{3,2,1,0:T(8,128)(2,1)S(1)} %bitcast.2), custom_call_target="tpu_custom_call" | custom-call | tf_op jit(solution)/shard_map/fold/pallas_call | solution.py:351
  462.0 0.7 copy.19
  (2 shorter events, 0.0 us)
Async XLA Ops:
  399.8 1.9 copy-start
where the time goes:
time: 463 us
  Pallas kernels  449 us (97%)
  other arithmetic  8.21 us (2%)
  local copies, waits for them, and re-layouts  5.04 us (1%)
    pallas_call x1, Pallas kernels, shards(): pl.pallas_call(spread, out_shape=(gate_shape, gate_shape, down_shape, far...  334 us
    pallas_call x1, Pallas kernels, shards(): pl.pallas_call(functools.partial(fold, chunks), out_shape=jax.ShapeDtypeS...  60.3 us
    pallas_call x1, Pallas kernels, shards(): pl.pallas_call(apply_experts, grid=(experts, units // block), out_shape=(...  54.9 us

commit v1 on v0

v1 whole, which is shorter than its diff:
```python
import functools

import jax
import jax.numpy as jnp
from jax import lax
from jax.experimental import pallas as pl
from jax.experimental.pallas import tpu as pltpu
from jax.sharding import PartitionSpec as P

EPS = 0.5
MESH = pl.DeviceIdType.MESH
VMEM_LIMIT = 63 * 1024 * 1024


def expert_rows(x, weight, wide, tall, total, expert):
    rows = x.shape[0]
    tile = rows // 2

    def step(i, carry):
        at = pl.ds(pl.multiple_of(i * tile, tile), tile)
        mine = x[at, :]
        gate_val = jnp.dot(mine, wide[0], preferred_element_type=jnp.float32)
        up_val = jnp.dot(mine, wide[1], preferred_element_type=jnp.float32)
        hidden = (jax.nn.silu(gate_val) * up_val).astype(jnp.bfloat16)
        result = jnp.dot(hidden, tall[...], preferred_element_type=jnp.float32)
        shares = weight[at, :]
        lane = lax.broadcasted_iota(jnp.int32, shares.shape, 1)
        share = jnp.sum(jnp.where(lane == expert, shares, 0.0), axis=1, keepdims=True)
        total[at, :] += share * result
        return carry

    lax.fori_loop(0, rows // tile, step, 0)


def spread(
    cuts, special,
    gain, tokens, routes, logit, gate_f32, up_f32, down_f32,
    gate_all, up_all, down_all, x_out, weight_out, total_out,
    own, far, down, stage, down_stage, x, weight, total, wide, tall,
    load, across_send, across_recv, near_send, near_recv, far_send, twin_send, twin_recv,
    onward_send, down_send, down_recv, local_sem, fetch_sem,
):
    _, blocks, depth, both = own.shape
    experts = blocks // cuts
    features, units = gate_all.shape[1:]
    block = units // cuts
    per = both // block
    fs, tp = lax.axis_index("fs"), lax.axis_index("tp")
    half, side = tp // 2, tp % 2
    twin = half * 2 + 1 - side
    col = down.shape[2]
    group = fs // per
    relay_side = group % 2
    lands = side != relay_side
    beyond = (1 - half) * 2
    apart = group // 2 != half
    close = group // 2 == half
    full = (gate_all, up_all)

    def remote(src, dst, send, recv, fs_to, tp_to):
        return pltpu.make_async_remote_copy(
            src_ref=src, dst_ref=dst, send_sem=send, recv_sem=recv,
            device_id=(fs_to, tp_to), device_id_type=MESH,
        )

    def columns(owner):
        return pl.ds(pl.multiple_of(owner * col, col), col)

    def slab(v):
        return v // cuts, pl.ds(pl.multiple_of(v % cuts * block, block), block)

    def only(condition, needed, action):
        if needed:
            pl.when(condition)(action)
        else:
            action()

    pieces = [(a, v) for v in range(blocks) for a in range(2)]
    early, late = pieces[:special], pieces[special : 2 * special]
    rows = pl.ds(pl.multiple_of(fs * depth, depth), depth)

    def crossing(a, v):
        return remote(
            own.at[a, v], far.at[side, a, v], across_send.at[a, v], across_recv.at[side, a, v],
            fs, beyond + relay_side,
        )

    def deal(source, a, v, owner, sem):
        e, at = slab(v)
        for h in range(per):
            remote(
                source.at[:, pl.ds(h * block, block)],
                full[a].at[e, rows, at],
                sem,
                near_recv.at[a, v],
                owner * per + h,
                half * 2 + 1 - owner % 2,
            ).start()

    def fetch(n):
        a, v = pieces[n]
        for h in range(per):
            pltpu.make_async_copy(
                (gate_f32, up_f32)[a].at[
                    v // cuts, :, pl.ds(h * units + v % cuts * block, block)
                ],
                stage.at[n % 2, :, pl.ds(h * block, block)],
                load.at[n % 2],
            ).start()

    def fetched(n):
        pltpu.make_async_copy(stage.at[n % 2], stage.at[n % 2], load.at[n % 2]).wait()

    def fetch_down(e):
        return pltpu.make_async_copy(down_f32.at[e], down_stage.at[e % 2], load.at[2 + e % 2])

    def down_local(e):
        return pltpu.make_async_copy(
            down.at[e], down_all.at[e, :, columns(tp)], local_sem.at[4 + e]
        )

    def down_to(k, e):
        return remote(
            down.at[e], down_all.at[e, :, columns(tp)], down_send.at[k, e],
            down_recv.at[(0, 1 + side)[k], e], fs, (twin, beyond + relay_side)[k],
        )

    def down_pass(s, e):
        part = down_all.at[e, :, columns(beyond + s)]
        return remote(part, part, down_send.at[2 + s, e], down_recv.at[1 + s, e], fs, twin)

    tile = min(depth, 32)
    fetch(0)
    token_copy = pltpu.make_async_copy(tokens, x, local_sem.at[0])
    token_copy.start()
    spot = lax.broadcasted_iota(jnp.int32, (depth, depth), 0)
    lane = lax.broadcasted_iota(jnp.int32, (depth, depth), 1)
    factor = jnp.sum(jnp.where(spot == lane, gain[...], 0.0), axis=1, keepdims=True)
    weight[0:depth, :] = jnp.broadcast_to(factor, (depth, weight.shape[1]))
    for n, piece in enumerate(pieces):
        a, v = piece
        if n + 1 < len(pieces):
            fetch(n + 1)
        e = v // cuts
        if a == 0 and v % cuts == 0:
            fetch_down(e).start()
        fetched(n)

        def scale(i, carry, a=a, v=v, n=n):
            at = pl.ds(pl.multiple_of(i * tile, tile), tile)
            own[a, v, at, :] = (stage[n % 2, at, :] * weight[at, 0:1]).astype(own.dtype)
            return carry

        lax.fori_loop(0, depth // tile, scale, 0)
        only(close, piece in late, lambda: crossing(a, v).start())
        only(close, piece in early, lambda: deal(own.at[a, v], a, v, tp, near_send.at[a, v]))
        if a == 1 and v % cuts == cuts - 1:
            fetch_down(e).wait()
            short = min(units, 128)

            def narrow(i, carry, e=e):
                at = pl.ds(pl.multiple_of(i * short, short), short)
                down[e, at, :] = down_stage[e % 2, at, :].astype(down.dtype)
                return carry

            lax.fori_loop(0, units // short, narrow, 0)
            down_to(1, e).start()
            down_to(0, e).start()
            down_local(e).start()

    token_copy.wait()
    count = x.shape[0]
    strip = count // 8

    def normalise(i, carry):
        at = pl.ds(pl.multiple_of(i * strip, strip), strip)
        floats = x[at, :].astype(jnp.float32)
        x[at, :] = (
            floats * lax.rsqrt(jnp.mean(floats * floats, axis=1, keepdims=True) + EPS)
        ).astype(x.dtype)
        return carry

    lax.fori_loop(0, count // strip, normalise, 0)
    first = jax.nn.sigmoid(logit[0:1, :] - logit[1:2, :])
    expert_of = lax.broadcasted_iota(jnp.int32, (weight.shape[1], count), 0)
    by_expert = jnp.where(routes[0:1, :] == expert_of, first, 0.0) + jnp.where(
        routes[1:2, :] == expert_of, 1.0 - first, 0.0
    )
    weight[...] = by_expert.T
    total[...] = jnp.zeros_like(total)
    x_copy = pltpu.make_async_copy(x, x_out, local_sem.at[1])
    x_copy.start()
    weight_copy = pltpu.make_async_copy(weight, weight_out, local_sem.at[2])
    weight_copy.start()

    def relay(a, v):
        for s in range(2):
            part = far.at[s, a, v]
            pltpu.make_async_copy(part, part, across_recv.at[s, a, v]).wait()
            deal(part, a, v, beyond + s, far_send.at[s, a, v])

    def relay_down(e):
        for s in range(2):
            down_pass(s, e).wait_recv()
            down_pass(s, e).start()

    away = pl.ds(pl.multiple_of((1 - group // 2) * (features // 2), features // 2), features // 2)

    def hand(a, v):
        e, at = slab(v)
        part = full[a].at[e, :, at]
        return remote(part, part, twin_send.at[a, v], twin_recv.at[a, v], fs, twin)

    def onward(a, v):
        e, at = slab(v)
        part = full[a].at[e, away, at]
        return remote(part, part, onward_send.at[a, v], near_recv.at[a, v], fs, beyond + side)

    def take(a, v, forward):
        e, at = slab(v)
        part = full[a].at[e, :, at]
        pltpu.make_async_copy(part, part, near_recv.at[a, v]).wait()
        if forward:
            onward(a, v).start()
        hand(a, v).start()

    def take_all(group_of, forward):
        for a, v in group_of:
            take(a, v, forward)

    @pl.when(jnp.logical_not(lands))
    def _():
        for a, v in pieces[: 2 * special]:
            only(apart, (a, v) in late, functools.partial(relay, a, v))
            if a == 1 and v % cuts == cuts - 1:
                relay_down(v // cuts)

        def pass_on(v, carry):
            relay(0, v)
            relay(1, v)
            pl.when(v % cuts == cuts - 1)(lambda: relay_down(v // cuts))
            return carry

        lax.fori_loop(special, blocks, pass_on, 0)

    @pl.when(lands)
    def _():
        pl.when(close)(lambda: take_all(late, True))
        pl.when(apart)(lambda: take_all(early, True))

    def arrive(v):
        @pl.when(lands)
        def _():
            take(0, v, False)
            take(1, v, False)

        @pl.when(jnp.logical_not(lands))
        def _():
            hand(0, v).wait_recv()
            hand(1, v).wait_recv()

    def down_ready(e):
        down_local(e).wait()
        down_to(0, e).wait_recv()

        @pl.when(lands)
        def _():
            for s in range(2):
                down_pass(s, e).wait_recv()

    def compute(v):
        e, at = slab(v)
        copies = [
            pltpu.make_async_copy(gate_all.at[e, :, at], wide.at[0], fetch_sem.at[0]),
            pltpu.make_async_copy(up_all.at[e, :, at], wide.at[1], fetch_sem.at[1]),
            pltpu.make_async_copy(down_all.at[e, at, :], tall, fetch_sem.at[2]),
        ]
        for copy in copies:
            copy.start()
        for copy in copies:
            copy.wait()
        expert_rows(x, weight, wide, tall, total, e)

    for e in range(special // cuts):
        down_ready(e)

    def turn(v, carry):
        arrive(v)
        pl.when(jnp.logical_or(v % cuts == 0, v == special))(lambda: down_ready(v // cuts))
        compute(v)
        return carry

    lax.fori_loop(special, blocks - 1, turn, 0)
    total_copy = pltpu.make_async_copy(total, total_out, local_sem.at[3])
    total_copy.start()
    if (blocks - 1) // cuts != (blocks - 2) // cuts:
        down_ready(experts - 1)

    @pl.when(lands)
    def _():
        take_all(pieces[-2:], False)
        pl.when(close)(lambda: take_all(early, False))
        pl.when(apart)(lambda: take_all(late, False))
        for a, v in pieces:
            hand(a, v).wait_send()

        def sent(group_of):
            for a, v in group_of:
                onward(a, v).wait_send()

        pl.when(close)(lambda: sent(late))
        pl.when(apart)(lambda: sent(early))

    @pl.when(jnp.logical_not(lands))
    def _():
        for a, v in pieces[: 2 * special] + pieces[-2:]:
            hand(a, v).wait_recv()
        for s in range(2):
            for a, v in pieces:
                gone = functools.partial(
                    pltpu.make_async_copy, far.at[s, a, v], far.at[s, a, v], far_send.at[s, a, v]
                )
                only(apart, (a, v) in late, lambda gone=gone: gone().wait())
            for e in range(experts):
                down_pass(s, e).wait_send()

    for piece in pieces:
        a, v = piece

        def dealt(sem, a=a, v=v):
            pltpu.make_async_copy(own.at[a, v], own.at[a, v], sem).wait()

        only(close, piece in late, lambda: crossing(a, v).wait_send())
        only(close, piece in early, lambda: dealt(near_send.at[a, v]))
    for e in range(experts):
        down_to(0, e).wait_send()
        down_to(1, e).wait_send()
    x_copy.wait()
    weight_copy.wait()
    total_copy.wait()


def finish(
    cuts, special,
    gate_all, up_all, down_all, x_in, weight_in, total_in,
    gate_out, up_out, down_out, part,
    wide, tall, x, weight, total, take_sem, put_sem, side_sem,
):
    slots = wide.shape[0]
    units = gate_all.shape[2]
    block = units // cuts
    blocks = gate_all.shape[0] * cuts
    turns = blocks // 2

    def place(s):
        i = s // 2
        mine = jnp.where(i == turns - 1, blocks - 1, i)
        v = jnp.where(s % 2 == 0, mine, special + i)
        return v // cuts, pl.ds(pl.multiple_of(v % cuts * block, block), block)

    def pull(s):
        e, at = place(s)
        slot = s % slots
        return [
            pltpu.make_async_copy(gate_all.at[e, :, at], wide.at[slot, 0], take_sem.at[slot, 0]),
            pltpu.make_async_copy(up_all.at[e, :, at], wide.at[slot, 1], take_sem.at[slot, 1]),
            pltpu.make_async_copy(down_all.at[e, at, :], tall.at[slot], take_sem.at[slot, 2]),
        ]

    def push(s):
        e, at = place(s)
        slot = s % slots
        return [
            pltpu.make_async_copy(wide.at[slot, 0], gate_out.at[e, :, at], put_sem.at[slot, 0]),
            pltpu.make_async_copy(wide.at[slot, 1], up_out.at[e, :, at], put_sem.at[slot, 1]),
            pltpu.make_async_copy(tall.at[slot], down_out.at[e, at, :], put_sem.at[slot, 2]),
        ]

    def start(copies):
        for copy in copies:
            copy.start()

    def wait(copies):
        for copy in copies:
            copy.wait()

    sides = [
        pltpu.make_async_copy(x_in, x, side_sem.at[0]),
        pltpu.make_async_copy(weight_in, weight, side_sem.at[1]),
        pltpu.make_async_copy(total_in, total, side_sem.at[2]),
    ]
    start(pull(0))
    start(sides)
    start(pull(1))
    wait(sides)

    def turn(i, carry):
        for s in (2 * i, 2 * i + 1):
            wait(pull(s))
            start(push(s))

        @pl.when(i >= 1)
        def _():
            wait(push(2 * i - 2))
            wait(push(2 * i - 1))

        @pl.when(i + 1 < turns)
        def _():
            start(pull(2 * i + 2))
            start(pull(2 * i + 3))

        slot = 2 * i % slots
        expert_rows(x, weight, wide.at[slot], tall.at[slot], total, place(2 * i)[0])
        return carry

    lax.fori_loop(0, turns, turn, 0)
    part[...] = total[...].astype(part.dtype)
    wait(push(blocks - 2))
    wait(push(blocks - 1))


def fold(chunks, part, out, low_in, mid, high_in, low_send, low_recv, high_send, high_recv):
    highs, _, rows, width = part.shape
    step = width // chunks
    fs, tp = lax.axis_index("fs"), lax.axis_index("tp")
    high, low = fs // 2, fs % 2
    first = []
    for k in range(chunks):
        copy = pltpu.make_async_remote_copy(
            src_ref=part.at[:, 1 - low, :, pl.ds(k * step, step)],
            dst_ref=low_in.at[k],
            send_sem=low_send.at[k],
            recv_sem=low_recv.at[k],
            device_id=(high * 2 + 1 - low, tp),
            device_id_type=MESH,
        )
        copy.start()
        first.append(copy)
    second = []
    for k in range(chunks):
        first[k].wait_recv()
        mid[k] = (
            part[:, low, :, pl.ds(k * step, step)].astype(jnp.float32)
            + low_in[k].astype(jnp.float32)
        ).astype(mid.dtype)
        for shift in range(1, highs):
            to = lax.rem(high + shift, highs)
            copy = pltpu.make_async_remote_copy(
                src_ref=mid.at[k, to],
                dst_ref=high_in.at[k, shift],
                send_sem=high_send.at[k, shift],
                recv_sem=high_recv.at[k, shift],
                device_id=(to * 2 + low, tp),
                device_id_type=MESH,
            )
            copy.start()
            second.append((k, copy))
    for k in range(chunks):
        total = part[high, low, :, pl.ds(k * step, step)].astype(jnp.float32) + low_in[
            k, high
        ].astype(jnp.float32)
        shift = 0
        for at, copy in second:
            if at == k:
                shift += 1
                copy.wait_recv()
                total = total + high_in[k, shift].astype(jnp.float32)
        out[:, pl.ds(k * step, step)] = total.astype(out.dtype)
    for copy in first:
        copy.wait_send()
    for _, copy in second:
        copy.wait_send()


def shards(fs_size, tokens, norm_gain, gate_weight, up_weight, down_weight, routes, route_logit):
    experts, depth, width = gate_weight.shape
    _, units, col = down_weight.shape
    rows, features = tokens.shape
    half = jnp.bfloat16
    anywhere = pl.BlockSpec(memory_space=pl.ANY)
    vmem = pl.BlockSpec(memory_space=pltpu.VMEM)
    dma = pltpu.SemaphoreType.DMA
    block = min(units, 512)
    cuts = units // block
    blocks = experts * cuts
    special = blocks // 2 - 1
    both = width // cuts
    gate_shape = jax.ShapeDtypeStruct((experts, features, units), half)
    down_shape = jax.ShapeDtypeStruct((experts, units, features), half)
    gate_all, up_all, down_all, x, weight, total = pl.pallas_call(
        functools.partial(spread, cuts, special),
        out_shape=(
            gate_shape, gate_shape, down_shape,
            jax.ShapeDtypeStruct((rows, features), half),
            jax.ShapeDtypeStruct((rows, 128), jnp.float32),
            jax.ShapeDtypeStruct((rows, features), jnp.float32),
        ),
        in_specs=[vmem, anywhere, vmem, vmem] + [anywhere] * 3,
        out_specs=(anywhere,) * 6,
        scratch_shapes=[
            pltpu.VMEM((2, blocks, depth, both), half),
            pltpu.VMEM((2, 2, blocks, depth, both), half),
            pltpu.VMEM((experts, units, col), half),
            pltpu.VMEM((2, depth, both), jnp.float32),
            pltpu.VMEM((2, units, col), jnp.float32),
            pltpu.VMEM((rows, features), half),
            pltpu.VMEM((rows, 128), jnp.float32),
            pltpu.VMEM((rows, features), jnp.float32),
            pltpu.VMEM((2, features, block), half),
            pltpu.VMEM((block, features), half),
            dma((4,)),
        ]
        + [dma((2, blocks)), dma((2, 2, blocks))]
        + [dma((2, blocks))] * 2
        + [dma((2, 2, blocks))]
        + [dma((2, blocks))] * 3
        + [dma((4, experts)), dma((3, experts))]
        + [dma((4 + experts,)), dma((3,))],
        compiler_params=pltpu.CompilerParams(
            has_side_effects=True, vmem_limit_bytes=VMEM_LIMIT
        ),
        name="spread",
    )(norm_gain[None, :], tokens, routes.T, route_logit.T, gate_weight, up_weight, down_weight)

    gate_out, up_out, down_out, part = pl.pallas_call(
        functools.partial(finish, cuts, special),
        out_shape=(
            gate_shape, gate_shape, down_shape, jax.ShapeDtypeStruct((rows, features), half),
        ),
        in_specs=[anywhere] * 6,
        out_specs=(anywhere,) * 3 + (vmem,),
        scratch_shapes=[
            pltpu.VMEM((4, 2, features, block), half),
            pltpu.VMEM((4, block, features), half),
            pltpu.VMEM((rows, features), half),
            pltpu.VMEM((rows, 128), jnp.float32),
            pltpu.VMEM((rows, features), jnp.float32),
            dma((4, 3)), dma((4, 3)), dma((3,)),
        ],
        compiler_params=pltpu.CompilerParams(vmem_limit_bytes=VMEM_LIMIT),
        name="finish",
    )(gate_all, up_all, down_all, x, weight, total)

    highs, mine, chunks = fs_size // 2, rows // fs_size, 8
    step = features // chunks
    mixed = pl.pallas_call(
        functools.partial(fold, chunks),
        out_shape=jax.ShapeDtypeStruct((mine, features), half),
        in_specs=[vmem],
        out_specs=vmem,
        scratch_shapes=[pltpu.VMEM((chunks, highs, mine, step), half)] * 3
        + [dma((chunks,))] * 2
        + [dma((chunks, highs))] * 2,
        compiler_params=pltpu.CompilerParams(
            has_side_effects=True, vmem_limit_bytes=VMEM_LIMIT // 2
        ),
        name="fold",
    )(part.reshape(highs, 2, mine, features))
    return (gate_out, up_out, down_out, mixed)


def solution(mesh):
    return jax.shard_map(
        functools.partial(shards, mesh.shape["fs"]),
        mesh=mesh,
        in_specs=(
            P("tp", None),
            P("fs"),
            P(None, "fs", "tp"),
            P(None, "fs", "tp"),
            P(None, "fs", "tp"),
            P("tp", None),
            P("tp", None),
        ),
        out_specs=(
            P(None, None, "fs"),
            P(None, None, "fs"),
            P(None, "fs", None),
            P(("tp", "fs"), None),
        ),
        check_vma=False,
    )
```

time: 463 us -> 439 us (0.948)
  Pallas kernels: 449 us -> 436 us
  other arithmetic: 8.21 us -> 0 us
    pallas_call x2, Pallas kernels: 389 us -> 361 us  [the longest x1 319 us: shards(): pl.pallas_call(functools.partial(spread, cuts, special), out_shape=(gate_...]
    pallas_call x1, Pallas kernels: 60.3 us -> 74.8 us  [shards(): pl.pallas_call(functools.partial(fold, chunks), out_shape=jax.ShapeDtypeS...]
where the time goes in v1:
time: 439 us
  Pallas kernels  436 us (99%)
    pallas_call x1, Pallas kernels, shards(): pl.pallas_call(functools.partial(spread, cuts, special), out_shape=(gate_...  319 us
    pallas_call x1, Pallas kernels, shards(): pl.pallas_call(functools.partial(fold, chunks), out_shape=jax.ShapeDtypeS...  74.8 us
    pallas_call x1, Pallas kernels, shards(): pl.pallas_call(functools.partial(finish, cuts, special), out_shape=(gate_...  41.5 us

profile of v1, /device:TPU:0, one launch (start us, length us, event | category | flops | bytes accessed | tf_op | source)
XLA Modules:
  0.0 438.8 jit_solution(17670602625702828767)
XLA Ops:
  0.6 319.3 %spread.1 = (bf16[4,2048,1024]{2,1,0:T(8,128)(2,1)}, bf16[4,2048,1024]{2,1,0:T(8,128)(2,1)}, bf16[4,1024,2048]{2,1,0:T(8,128)(2,1)}, bf16[768,2048]{1,0:T(8,128)...) custom-call(f32[1,256]{1,0:T(1,128)} %bitcast.7, bf16[768,2048]{1,0:T(8,128)(2,1)} %tokens.1, s32[2,768]{1,0:T(2,128)} %bitcast.5, ...), custom_call_target="tpu_custom_call" | custom-call | tf_op jit(solution)/shard_map/spread/pallas_call | solution.py:490
  319.9 41.5 %finish.1 = (bf16[4,2048,1024]{2,1,0:T(8,128)(2,1)}, bf16[4,2048,1024]{2,1,0:T(8,128)(2,1)}, bf16[4,1024,2048]{2,1,0:T(8,128)(2,1)}, bf16[768,2048]{1,0:T(8,128)(2,1)}) custom-call(bf16[4,2048,1024]{2,1,0:T(8,128)(2,1)} %get-tuple-element.14.gate_all, bf16[4,2048,1024]{2,1,0:T(8,128)(2,1)} %get-tuple-element.15.up_all, ...), custom_call_target="tpu_custom_call" | custom-call | tf_op jit(solution)/shard_map/finish/pallas_call | solution.py:525
  361.4 0.0 copy-start
  361.4 1.9 copy-done
  363.3 74.8 %fold.1 = bf16[96,2048]{1,0:T(8,128)(2,1)S(1)} custom-call(bf16[4,2,96,2048]{3,2,1,0:T(8,128)(2,1)S(1)} %bitcast.4), custom_call_target="tpu_custom_call" | custom-call | tf_op jit(solution)/shard_map/fold/pallas_call | solution.py:546
  438.1 0.7 copy.12
Async XLA Ops:
  361.4 1.9 copy-start

commit v2 on v1

v2 whole, which is shorter than its diff:
```python
import functools

import jax
import jax.numpy as jnp
from jax import lax
from jax.experimental import pallas as pl
from jax.experimental.pallas import tpu as pltpu
from jax.sharding import PartitionSpec as P

EPS = 0.5
MESH = pl.DeviceIdType.MESH
VMEM_LIMIT = 63 * 1024 * 1024


def expert_tile(x, weight, wide, tall, total, expert, at):
    mine = x[at, :]
    gate_val = jnp.dot(mine, wide[0], preferred_element_type=jnp.float32)
    up_val = jnp.dot(mine, wide[1], preferred_element_type=jnp.float32)
    hidden = (jax.nn.silu(gate_val) * up_val).astype(jnp.bfloat16)
    result = jnp.dot(hidden, tall[...], preferred_element_type=jnp.float32)
    shares = weight[at, :]
    lane = lax.broadcasted_iota(jnp.int32, shares.shape, 1)
    share = jnp.sum(jnp.where(lane == expert, shares, 0.0), axis=1, keepdims=True)
    total[at, :] += share * result


def expert_rows(x, weight, wide, tall, total, expert):
    rows = x.shape[0]
    tile = rows // 2

    def step(i, carry):
        at = pl.ds(pl.multiple_of(i * tile, tile), tile)
        expert_tile(x, weight, wide, tall, total, expert, at)
        return carry

    lax.fori_loop(0, rows // tile, step, 0)


def spread(
    cuts, special,
    gain, tokens, routes, logit, gate_f32, up_f32, down_f32,
    gate_all, up_all, down_all, far, mixed,
    own, down, stage, down_stage, x, weight, total, wide, tall, part, low_in, mid, high_in,
    load, across_send, across_recv, near_send, near_recv, far_send, twin_send, twin_recv,
    onward_send, down_send, down_recv, local_sem, fetch_sem,
    low_send, low_recv, high_send, high_recv,
):
    _, blocks, depth, both = own.shape
    experts = blocks // cuts
    features, units = gate_all.shape[1:]
    block = units // cuts
    per = both // block
    fs, tp = lax.axis_index("fs"), lax.axis_index("tp")
    half, side = tp // 2, tp % 2
    twin = half * 2 + 1 - side
    col = down.shape[2]
    group = fs // per
    relay_side = group % 2
    lands = side != relay_side
    beyond = (1 - half) * 2
    apart = group // 2 != half
    close = group // 2 == half
    full = (gate_all, up_all)

    def remote(src, dst, send, recv, fs_to, tp_to):
        return pltpu.make_async_remote_copy(
            src_ref=src, dst_ref=dst, send_sem=send, recv_sem=recv,
            device_id=(fs_to, tp_to), device_id_type=MESH,
        )

    def columns(owner):
        return pl.ds(pl.multiple_of(owner * col, col), col)

    def slab(v):
        return v // cuts, pl.ds(pl.multiple_of(v % cuts * block, block), block)

    def only(condition, needed, action):
        if needed:
            pl.when(condition)(action)
        else:
            action()

    lead = [(a, v) for v in range(special) for a in range(2)]
    early, late = lead[:special], lead[special:]
    split, final = (0, blocks - 1), (1, blocks - 1)
    lead.append(split)
    middle = [(a, v) for v in range(special, blocks - 1) for a in range(2)]
    pieces = lead + middle + [final]
    ahead = list(range(special // cuts))
    after = {}
    for e in range(experts):
        inside = [n for n, (a, v) in enumerate(pieces[:-1]) if v // cuts == e and (a, v) in middle]
        after.setdefault(inside[-1] if inside else len(pieces) - 1, []).append(e)
    for e in ahead:
        after = {n: [i for i in held if i != e] for n, held in after.items()}
        after.setdefault(2 * cuts * (e + 1) - 1, []).append(e)
    kept = pl.ds(depth // 2, depth // 2)

    def crossing(a, v):
        return remote(
            own.at[a, v], far.at[side, a, v], across_send.at[a, v], across_recv.at[side, a, v],
            fs, beyond + relay_side,
        )

    def crossing_part(a, v):
        return remote(
            own.at[a, v, kept], far.at[side, a, v, kept], across_send.at[a, v],
            across_recv.at[side, a, v], fs, beyond + relay_side,
        )

    def deal(source, a, v, owner, sem, low=0):
        e, at = slab(v)
        rows = pl.ds(pl.multiple_of(fs * depth + low, depth - low), depth - low)
        for h in range(per):
            remote(
                source.at[:, pl.ds(h * block, block)],
                full[a].at[e, rows, at],
                sem,
                near_recv.at[a, v],
                owner * per + h,
                half * 2 + 1 - owner % 2,
            ).start()

    def fetch(n):
        a, v = pieces[n]
        for h in range(per):
            pltpu.make_async_copy(
                (gate_f32, up_f32)[a].at[
                    v // cuts, :, pl.ds(h * units + v % cuts * block, block)
                ],
                stage.at[n % 2, :, pl.ds(h * block, block)],
                load.at[n % 2],
            ).start()

    def fetched(n):
        pltpu.make_async_copy(stage.at[n % 2], stage.at[n % 2], load.at[n % 2]).wait()

    def fetch_down(e):
        return pltpu.make_async_copy(down_f32.at[e], down_stage.at[e % 2], load.at[2 + e % 2])

    def down_local(e):
        return pltpu.make_async_copy(
            down.at[e], down_all.at[e, :, columns(tp)], local_sem.at[4 + e]
        )

    def down_to(k, e):
        return remote(
            down.at[e], down_all.at[e, :, columns(tp)], down_send.at[k, e],
            down_recv.at[(0, 1 + side)[k], e], fs, (twin, beyond + relay_side)[k],
        )

    def down_pass(s, e):
        part = down_all.at[e, :, columns(beyond + s)]
        return remote(part, part, down_send.at[2 + s, e], down_recv.at[1 + s, e], fs, twin)

    tile = min(depth, 32)
    fetch(0)
    token_copy = pltpu.make_async_copy(tokens, x, local_sem.at[0])
    token_copy.start()
    spot = lax.broadcasted_iota(jnp.int32, (depth, depth), 0)
    lane = lax.broadcasted_iota(jnp.int32, (depth, depth), 1)
    factor = jnp.sum(jnp.where(spot == lane, gain[...], 0.0), axis=1, keepdims=True)
    weight[0:depth, :] = jnp.broadcast_to(factor, (depth, weight.shape[1]))
    for n, piece in enumerate(pieces):
        a, v = piece
        if n + 1 < len(pieces):
            fetch(n + 1)
        if n == 0:
            fetch_down(0).start()
            fetch_down(1).start()
        fetched(n)

        def scale(i, carry, a=a, v=v, n=n):
            at = pl.ds(pl.multiple_of(i * tile, tile), tile)
            own[a, v, at, :] = (stage[n % 2, at, :] * weight[at, 0:1]).astype(own.dtype)
            return carry

        lax.fori_loop(0, depth // tile, scale, 0)
        only(close, piece in late or piece == split, lambda: crossing(a, v).start())
        if piece == split:
            pl.when(apart)(lambda: crossing_part(a, v).start())
        only(close, piece in early, lambda: deal(own.at[a, v], a, v, tp, near_send.at[a, v]))
        for e in after.get(n, []):
            fetch_down(e).wait()
            short = min(units, 128)

            def narrow(i, carry, e=e):
                at = pl.ds(pl.multiple_of(i * short, short), short)
                down[e, at, :] = down_stage[e % 2, at, :].astype(down.dtype)
                return carry

            lax.fori_loop(0, units // short, narrow, 0)
            if e + 2 < experts:
                fetch_down(e + 2).start()
            down_to(1, e).start()
            down_to(0, e).start()
            down_local(e).start()

    token_copy.wait()
    count = x.shape[0]
    strip = count // 8

    def normalise(i, carry):
        at = pl.ds(pl.multiple_of(i * strip, strip), strip)
        floats = x[at, :].astype(jnp.float32)
        x[at, :] = (
            floats * lax.rsqrt(jnp.mean(floats * floats, axis=1, keepdims=True) + EPS)
        ).astype(x.dtype)
        return carry

    lax.fori_loop(0, count // strip, normalise, 0)
    first = jax.nn.sigmoid(logit[0:1, :] - logit[1:2, :])
    expert_of = lax.broadcasted_iota(jnp.int32, (weight.shape[1], count), 0)
    by_expert = jnp.where(routes[0:1, :] == expert_of, first, 0.0) + jnp.where(
        routes[1:2, :] == expert_of, 1.0 - first, 0.0
    )
    weight[...] = by_expert.T
    total[...] = jnp.zeros_like(total)

    def relay(a, v, low=0):
        for s in range(2):
            part = far.at[s, a, v, pl.ds(low, depth - low)]
            pltpu.make_async_copy(part, part, across_recv.at[s, a, v]).wait()
            deal(part, a, v, beyond + s, far_send.at[s, a, v], low)

    def relay_down(e):
        for s in range(2):
            down_pass(s, e).wait_recv()
            down_pass(s, e).start()

    away = pl.ds(pl.multiple_of((1 - group // 2) * (features // 2), features // 2), features // 2)

    def hand(a, v):
        e, at = slab(v)
        part = full[a].at[e, :, at]
        return remote(part, part, twin_send.at[a, v], twin_recv.at[a, v], fs, twin)

    sources = features // depth // 2

    def onward(a, v):
        e, at = slab(v)
        if (a, v) != split:
            part = full[a].at[e, away, at]
            remote(
                part, part, onward_send.at[a, v], near_recv.at[a, v], fs, beyond + side
            ).start()
        else:

            def send(i, carry):
                start = ((1 - group // 2) * sources + i) * depth
                part = full[a].at[e, pl.ds(pl.multiple_of(start, depth), depth // 2), at]
                remote(
                    part, part, onward_send.at[a, v], near_recv.at[a, v], fs, beyond + side
                ).start()
                return carry

            lax.fori_loop(0, sources, send, 0)

    def onward_sent(a, v):
        e, at = slab(v)
        count = features // (4 if (a, v) == split else 2)
        part = full[a].at[e, pl.ds(0, count), at]
        pltpu.make_async_copy(part, part, onward_send.at[a, v]).wait()

    def take(a, v, forward):
        e, at = slab(v)
        part = full[a].at[e, :, at]
        pltpu.make_async_copy(part, part, near_recv.at[a, v]).wait()
        if forward:
            onward(a, v)
        hand(a, v).start()

    def take_all(group_of, forward):
        for a, v in group_of:
            take(a, v, forward)

    @pl.when(jnp.logical_not(lands))
    def _():
        for n, (a, v) in enumerate(lead):
            only(apart, (a, v) in late or (a, v) == split, functools.partial(relay, a, v))
            if (a, v) == split:
                pl.when(close)(functools.partial(relay, a, v, depth // 2))
            for e in after.get(n, []):
                relay_down(e)

        def pass_on(v, carry):
            relay(0, v)
            relay(1, v)
            last = jnp.logical_or(v % cuts == cuts - 1, v == blocks - 2)
            pl.when(last)(lambda: relay_down(v // cuts))
            return carry

        lax.fori_loop(special, blocks - 1, pass_on, 0)
        relay(*final)
        for e in after.get(len(pieces) - 1, []):
            relay_down(e)

    moved = late + [split]

    @pl.when(lands)
    def _():
        pl.when(close)(lambda: take_all(moved, True))
        pl.when(apart)(lambda: take_all(early, True))

    def arrive(v):
        @pl.when(lands)
        def _():
            take(0, v, False)
            take(1, v, False)

        @pl.when(jnp.logical_not(lands))
        def _():
            hand(0, v).wait_recv()
            hand(1, v).wait_recv()

    def down_ready(e):
        down_local(e).wait()
        down_to(0, e).wait_recv()

        @pl.when(lands)
        def _():
            for s in range(2):
                down_pass(s, e).wait_recv()

    def bring(a, v, i):
        e, at = slab(v)
        return pltpu.make_async_copy(full[a].at[e, :, at], wide.at[i, a], fetch_sem.at[3 * i + a])

    def bring_down(v, i):
        e, at = slab(v)
        return pltpu.make_async_copy(down_all.at[e, at, :], tall.at[i], fetch_sem.at[3 * i + 2])

    def compute(v):
        e, at = slab(v)
        copies = [bring(0, v, 0), bring(1, v, 0), bring_down(v, 0)]
        for copy in copies:
            copy.start()
        for copy in copies:
            copy.wait()
        expert_rows(x, weight, wide.at[0], tall.at[0], total, e)

    for e in range(special // cuts):
        down_ready(e)

    def turn(v, carry):
        arrive(v)
        pl.when(jnp.logical_or(v % cuts == 0, v == special))(lambda: down_ready(v // cuts))
        compute(v)
        return carry

    lax.fori_loop(special, blocks - 1, turn, 0)

    @pl.when(jnp.logical_and(lands, close))
    def _():
        take_all(early, False)

    for v in range(special // 2):

        @pl.when(jnp.logical_not(lands))
        def _(v=v):
            hand(0, v).wait_recv()
            hand(1, v).wait_recv()

        compute(v)
    if (blocks - 1) // cuts != (blocks - 2) // cuts:
        down_ready(experts - 1)
    ends = list(range(special // 2, special)) + [blocks - 1]
    for i, v in enumerate(ends):
        bring_down(v, i).start()
    coming = [p for p in lead[special // 2 * 2 :] + [final]]

    @pl.when(jnp.logical_and(lands, apart))
    def _():
        take_all(moved, False)

    @pl.when(lands)
    def _():
        take_all([final], False)

    @pl.when(jnp.logical_not(lands))
    def _():
        for a, v in coming:
            hand(a, v).wait_recv()

    for a, v in coming:
        bring(a, v, ends.index(v)).start()
    for i, v in enumerate(ends):
        bring_down(v, i).wait()
        bring(0, v, i).wait()
        bring(1, v, i).wait()

    highs, _, owned, width = part.shape
    high, low = fs // 2, fs % 2
    tiles = min(highs, 4)
    held = highs // tiles
    span = count // tiles
    column = width // 2

    def tile_of(k):
        return lax.rem(high // held + k, tiles)

    def low_copy(k, c):
        t = tile_of(k)
        at, over = pl.ds(t * held, held), pl.ds(c * column, column)
        return remote(
            part.at[at, 1 - low, :, over], low_in.at[at, :, over],
            low_send.at[t, c], low_recv.at[t, c], high * 2 + 1 - low, tp,
        )

    def high_copy(shift, c):
        to = lax.rem(high + shift, highs)
        over = pl.ds(c * column, column)
        return remote(
            mid.at[to, :, over], high_in.at[shift, :, over],
            high_send.at[shift, c], high_recv.at[shift, c], to * 2 + low, tp,
        )

    def merge(k):
        t = tile_of(k)
        for c in range(2):
            over = pl.ds(c * column, column)
            low_copy(k, c).wait_recv()
            for n in range(held):
                to = t * held + n
                mid[to, :, over] = (
                    part[to, low, :, over].astype(jnp.float32)
                    + low_in[to, :, over].astype(jnp.float32)
                ).astype(mid.dtype)

                @pl.when(to != high)
                def _(to=to):
                    high_copy(lax.rem(to - high + highs, highs), c).start()

    def closing(k, carry):
        t = tile_of(k)
        at = pl.ds(pl.multiple_of(t * span, span), span)
        for i, v in enumerate(ends):
            expert_tile(x, weight, wide.at[i], tall.at[i], total, v // cuts, at)
        values = total[at, :]
        for n in range(held):
            for side_of in range(2):
                start = (n * 2 + side_of) * owned
                part[t * held + n, side_of] = values[start : start + owned].astype(part.dtype)
        for c in range(2):
            low_copy(k, c).start()
        pl.when(k >= 2)(lambda: merge(k - 1))
        return carry

    lax.fori_loop(1, tiles + 1, closing, 0)
    merge(tiles)
    for c in range(2):
        over = pl.ds(c * column, column)
        gathered = part[high, low, :, over].astype(jnp.float32) + low_in[high, :, over].astype(
            jnp.float32
        )
        for shift in range(1, highs):
            high_copy(shift, c).wait_recv()
            gathered = gathered + high_in[shift, :, over].astype(jnp.float32)
        mixed[:, over] = gathered.astype(mixed.dtype)
    for c in range(2):
        for k in range(tiles):
            low_copy(k, c).wait_send()
        for shift in range(1, highs):
            high_copy(shift, c).wait_send()

    @pl.when(lands)
    def _():
        for a, v in pieces:
            hand(a, v).wait_send()

        def sent(group_of):
            for a, v in group_of:
                onward_sent(a, v)

        pl.when(close)(lambda: sent(moved))
        pl.when(apart)(lambda: sent(early))

    @pl.when(jnp.logical_not(lands))
    def _():
        for s in range(2):
            for a, v in pieces:

                def gone(low, s=s, a=a, v=v):
                    part = far.at[s, a, v, pl.ds(low, depth - low)]
                    pltpu.make_async_copy(part, part, far_send.at[s, a, v]).wait()

                only(apart, (a, v) in moved, functools.partial(gone, 0))
                if (a, v) == split:
                    pl.when(close)(functools.partial(gone, depth // 2))
            for e in range(experts):
                down_pass(s, e).wait_send()

    for piece in pieces:
        a, v = piece

        def dealt(sem, a=a, v=v):
            pltpu.make_async_copy(own.at[a, v], own.at[a, v], sem).wait()

        only(close, piece in moved, lambda: crossing(a, v).wait_send())
        if piece == split:
            pl.when(apart)(lambda: crossing_part(a, v).wait_send())
        only(close, piece in early, lambda: dealt(near_send.at[a, v]))
    for e in range(experts):
        down_to(0, e).wait_send()
        down_to(1, e).wait_send()


def finish(gate_in, up_in, down_in, mixed_in, gate, up, down, mixed, ring, small, take, put, side):
    slots, rows, width = ring.shape
    steps = []
    for source, target in ((gate_in, gate), (up_in, up), (down_in, down)):
        experts, height, span = source.shape
        for e in range(experts):
            for r in range(0, height, min(height, rows)):
                for c in range(0, span, width):
                    at = (e, pl.ds(r, min(height, rows)), pl.ds(c, width))
                    steps.append((source.at[at], target.at[at], min(height, rows)))

    def pull(n):
        source, _, height = steps[n]
        slot = n % slots
        return pltpu.make_async_copy(source, ring.at[slot, pl.ds(0, height)], take.at[slot])

    def push(n):
        _, target, height = steps[n]
        slot = n % slots
        return pltpu.make_async_copy(ring.at[slot, pl.ds(0, height)], target, put.at[slot])

    ahead = slots // 2
    inward = pltpu.make_async_copy(mixed_in, small, side.at[0])
    inward.start()
    for n in range(min(ahead, len(steps))):
        pull(n).start()
    for n in range(len(steps)):
        if n + ahead < len(steps):
            if n + ahead >= slots:
                push(n + ahead - slots).wait()
            pull(n + ahead).start()
        pull(n).wait()
        push(n).start()
    inward.wait()
    outward = pltpu.make_async_copy(small, mixed, side.at[1])
    outward.start()
    for n in range(max(0, len(steps) - slots), len(steps)):
        push(n).wait()
    outward.wait()


def shards(fs_size, tokens, norm_gain, gate_weight, up_weight, down_weight, routes, route_logit):
    experts, depth, width = gate_weight.shape
    _, units, col = down_weight.shape
    rows, features = tokens.shape
    half = jnp.bfloat16
    anywhere = pl.BlockSpec(memory_space=pl.ANY)
    vmem = pl.BlockSpec(memory_space=pltpu.VMEM)
    dma = pltpu.SemaphoreType.DMA
    block = min(units, 512)
    cuts = units // block
    blocks = experts * cuts
    special = blocks // 2 - 1
    both = width // cuts
    gate_shape = jax.ShapeDtypeStruct((experts, features, units), half)
    down_shape = jax.ShapeDtypeStruct((experts, units, features), half)
    highs, owned = fs_size // 2, rows // fs_size
    tiles = min(highs, 4)
    last = special - special // 2 + 1
    mixed_shape = jax.ShapeDtypeStruct((owned, features), half)
    gate_all, up_all, down_all, _, summed = pl.pallas_call(
        functools.partial(spread, cuts, special),
        out_shape=(
            gate_shape, gate_shape, down_shape,
            jax.ShapeDtypeStruct((2, 2, blocks, depth, both), half),
            mixed_shape,
        ),
        in_specs=[vmem, anywhere, vmem, vmem] + [anywhere] * 3,
        out_specs=(anywhere,) * 4 + (vmem,),
        scratch_shapes=[
            pltpu.VMEM((2, blocks, depth, both), half),
            pltpu.VMEM((experts, units, col), half),
            pltpu.VMEM((2, depth, both), jnp.float32),
            pltpu.VMEM((2, units, col), jnp.float32),
            pltpu.VMEM((rows, features), half),
            pltpu.VMEM((rows, 128), jnp.float32),
            pltpu.VMEM((rows, features), jnp.float32),
            pltpu.VMEM((last, 2, features, block), half),
            pltpu.VMEM((last, block, features), half),
            pltpu.VMEM((highs, 2, owned, features), half),
            pltpu.VMEM((highs, owned, features), half),
            pltpu.VMEM((highs, owned, features), half),
            pltpu.VMEM((highs, owned, features), half),
            dma((4,)),
        ]
        + [dma((2, blocks)), dma((2, 2, blocks))]
        + [dma((2, blocks))] * 2
        + [dma((2, 2, blocks))]
        + [dma((2, blocks))] * 3
        + [dma((4, experts)), dma((3, experts))]
        + [dma((4 + experts,)), dma((3 * last,))]
        + [dma((tiles, 2))] * 2
        + [dma((highs, 2))] * 2,
        compiler_params=pltpu.CompilerParams(
            has_side_effects=True, vmem_limit_bytes=VMEM_LIMIT
        ),
        name="spread",
    )(norm_gain[None, :], tokens, routes.T, route_logit.T, gate_weight, up_weight, down_weight)

    slots = 8
    gate_out, up_out, down_out, mixed = pl.pallas_call(
        finish,
        out_shape=(gate_shape, gate_shape, down_shape, mixed_shape),
        in_specs=[anywhere] * 4,
        out_specs=(anywhere,) * 4,
        scratch_shapes=[
            pltpu.VMEM((slots, features, units), half),
            pltpu.VMEM((owned, features), half),
            dma((slots,)), dma((slots,)), dma((2,)),
        ],
        compiler_params=pltpu.CompilerParams(vmem_limit_bytes=VMEM_LIMIT),
        name="finish",
    )(gate_all, up_all, down_all, summed)
    return (gate_out, up_out, down_out, mixed)


def solution(mesh):
    return jax.shard_map(
        functools.partial(shards, mesh.shape["fs"]),
        mesh=mesh,
        in_specs=(
            P("tp", None),
            P("fs"),
            P(None, "fs", "tp"),
            P(None, "fs", "tp"),
            P(None, "fs", "tp"),
            P("tp", None),
            P("tp", None),
        ),
        out_specs=(
            P(None, None, "fs"),
            P(None, None, "fs"),
            P(None, "fs", None),
            P(("tp", "fs"), None),
        ),
        check_vma=False,
    )
```

time: 439 us -> 411 us (0.936)
  Pallas kernels: 436 us -> 406 us
    pallas_call x2 -> x1, Pallas kernels: 116 us -> 33.3 us  [shards(): pl.pallas_call(finish, out_shape=(gate_shape, gate_shape, down_shape, mix...]
    pallas_call x1, Pallas kernels: 319 us -> 373 us  [shards(): pl.pallas_call(functools.partial(spread, cuts, special), out_shape=(gate_...]
where the time goes in v2:
time: 411 us; the launch traced here: 407 us
  Pallas kernels  406 us (99%)
    pallas_call x1, Pallas kernels, shards(): pl.pallas_call(functools.partial(spread, cuts, special), out_shape=(gate_...  373 us
    pallas_call x1, Pallas kernels, shards(): pl.pallas_call(finish, out_shape=(gate_shape, gate_shape, down_shape, mix...  33.3 us

profile of v2, /device:TPU:0, one launch (start us, length us, event | category | flops | bytes accessed | tf_op | source)
XLA Modules:
  0.0 407.1 jit_solution(7752582062707169304)
XLA Ops:
  0.6 373.2 %spread.1 = (bf16[4,2048,1024]{2,1,0:T(8,128)(2,1)}, bf16[4,2048,1024]{2,1,0:T(8,128)(2,1)}, bf16[4,1024,2048]{2,1,0:T(8,128)(2,1)}, bf16[2,2,8,256,1024]{4,3,2,1,0:T(8,128)(2,1)}, bf16[96,2048]{1,0:T(8,128)(2,1)}) custom-call(f32[1,256]{1,0:T(1,128)} %bitcast.5, bf16[768,2048]{1,0:T(8,128)(2,1)} %tokens.1, s32[2,768]{1,0:T(2,128)} %bitcast.3, ...), custom_call_target="tpu_custom_call" | custom-call | tf_op jit(solution)/shard_map/spread/pallas_call | solution.py:568
  373.8 33.3 %finish.1 = (bf16[4,2048,1024]{2,1,0:T(8,128)(2,1)}, bf16[4,2048,1024]{2,1,0:T(8,128)(2,1)}, bf16[4,1024,2048]{2,1,0:T(8,128)(2,1)}, bf16[96,2048]{1,0:T(8,128)(2,1)}) custom-call(bf16[4,2048,1024]{2,1,0:T(8,128)(2,1)} %get-tuple-element.8.gate_in, bf16[4,2048,1024]{2,1,0:T(8,128)(2,1)} %get-tuple-element.9.up_in, ...), custom_call_target="tpu_custom_call" | custom-call | tf_op jit(solution)/shard_map/finish/pallas_call | solution.py:608

commit v3 on v2

--- a/solution.py
+++ b/solution.py
@@ -8,6 +8,7 @@
 from jax.sharding import PartitionSpec as P
 
 EPS = 0.5
+QUARTERS = 1
 MESH = pl.DeviceIdType.MESH
 VMEM_LIMIT = 63 * 1024 * 1024
 
@@ -37,7 +38,7 @@
 
 
 def spread(
-    cuts, special,
+    cuts, special, fs_size, tp_size,
     gain, tokens, routes, logit, gate_f32, up_f32, down_f32,
     gate_all, up_all, down_all, far, mixed,
     own, down, stage, down_stage, x, weight, total, wide, tall, part, low_in, mid, high_in,
@@ -94,7 +95,8 @@
     for e in ahead:
         after = {n: [i for i in held if i != e] for n, held in after.items()}
         after.setdefault(2 * cuts * (e + 1) - 1, []).append(e)
-    kept = pl.ds(depth // 2, depth // 2)
+    moving = depth * QUARTERS // 4
+    kept = pl.ds(moving, depth - moving)
 
     def crossing(a, v):
         return remote(
@@ -110,7 +112,7 @@
 
     def deal(source, a, v, owner, sem, low=0):
         e, at = slab(v)
-        rows = pl.ds(pl.multiple_of(fs * depth + low, depth - low), depth - low)
+        rows = pl.ds(pl.multiple_of(fs * depth + low, low or depth), depth - low)
         for h in range(per):
             remote(
                 source.at[:, pl.ds(h * block, block)],
@@ -153,7 +155,31 @@
         part = down_all.at[e, :, columns(beyond + s)]
         return remote(part, part, down_send.at[2 + s, e], down_recv.at[1 + s, e], fs, twin)
 
+    def relay(a, v, low=0):
+        for s in range(2):
+            part = far.at[s, a, v, pl.ds(low, depth - low)]
+            pltpu.make_async_copy(part, part, across_recv.at[s, a, v]).wait()
+            deal(part, a, v, beyond + s, far_send.at[s, a, v], low)
+
+    met = pltpu.get_barrier_semaphore()
+
+    def greet():
+        def signal(i, carry):
+            to = lax.rem(fs * tp_size + tp + i, fs_size * tp_size)
+            pl.semaphore_signal(
+                met, inc=1, device_id=(to // tp_size, to % tp_size), device_id_type=MESH
+            )
+            return carry
+
+        lax.fori_loop(1, fs_size * tp_size, signal, 0)
+
+    def meet():
+        pl.semaphore_wait(met, fs_size * tp_size - 1)
+
+    turns = {len(pieces) // 2 + 3 * i: piece for i, piece in enumerate(early)}
+
     tile = min(depth, 32)
+    greet()
     fetch(0)
     token_copy = pltpu.make_async_copy(tokens, x, local_sem.at[0])
     token_copy.start()
@@ -169,6 +195,8 @@
             fetch_down(0).start()
             fetch_down(1).start()
         fetched(n)
+        if n == 0:
+            meet()
 
         def scale(i, carry, a=a, v=v, n=n):
             at = pl.ds(pl.multiple_of(i * tile, tile), tile)
@@ -195,6 +223,11 @@
             down_to(1, e).start()
             down_to(0, e).start()
             down_local(e).start()
+        if n in turns:
+            pl.when(jnp.logical_not(lands))(functools.partial(relay, *turns[n]))
+    for n, piece in turns.items():
+        if n >= len(pieces):
+            pl.when(jnp.logical_not(lands))(functools.partial(relay, *piece))
 
     token_copy.wait()
     count = x.shape[0]
@@ -217,12 +250,6 @@
     weight[...] = by_expert.T
     total[...] = jnp.zeros_like(total)
 
-    def relay(a, v, low=0):
-        for s in range(2):
-            part = far.at[s, a, v, pl.ds(low, depth - low)]
-            pltpu.make_async_copy(part, part, across_recv.at[s, a, v]).wait()
-            deal(part, a, v, beyond + s, far_send.at[s, a, v], low)
-
     def relay_down(e):
         for s in range(2):
             down_pass(s, e).wait_recv()
@@ -248,7 +275,7 @@
 
             def send(i, carry):
                 start = ((1 - group // 2) * sources + i) * depth
-                part = full[a].at[e, pl.ds(pl.multiple_of(start, depth), depth // 2), at]
+                part = full[a].at[e, pl.ds(pl.multiple_of(start, depth), moving), at]
                 remote(
                     part, part, onward_send.at[a, v], near_recv.at[a, v], fs, beyond + side
                 ).start()
@@ -258,7 +285,7 @@
 
     def onward_sent(a, v):
         e, at = slab(v)
-        count = features // (4 if (a, v) == split else 2)
+        count = sources * (moving if (a, v) == split else depth)
         part = full[a].at[e, pl.ds(0, count), at]
         pltpu.make_async_copy(part, part, onward_send.at[a, v]).wait()
 
@@ -277,23 +304,12 @@
     @pl.when(jnp.logical_not(lands))
     def _():
         for n, (a, v) in enumerate(lead):
-            only(apart, (a, v) in late or (a, v) == split, functools.partial(relay, a, v))
+            if (a, v) not in early:
+                pl.when(apart)(functools.partial(relay, a, v))
             if (a, v) == split:
-                pl.when(close)(functools.partial(relay, a, v, depth // 2))
+                pl.when(close)(functools.partial(relay, a, v, moving))
             for e in after.get(n, []):
                 relay_down(e)
-
-        def pass_on(v, carry):
-            relay(0, v)
-            relay(1, v)
-            last = jnp.logical_or(v % cuts == cuts - 1, v == blocks - 2)
-            pl.when(last)(lambda: relay_down(v // cuts))
-            return carry
-
-        lax.fori_loop(special, blocks - 1, pass_on, 0)
-        relay(*final)
-        for e in after.get(len(pieces) - 1, []):
-            relay_down(e)
 
     moved = late + [split]
 
@@ -342,13 +358,34 @@
     for e in range(special // cuts):
         down_ready(e)
 
+    def pass_on(v):
+        @pl.when(v < blocks - 1)
+        def _():
+            relay(0, v)
+            relay(1, v)
+            last = jnp.logical_or(v % cuts == cuts - 1, v == blocks - 2)
+            pl.when(last)(lambda: relay_down(v // cuts))
+
+        @pl.when(v == blocks - 1)
+        def _():
+            relay(*final)
+            for e in after.get(len(pieces) - 1, []):
+                relay_down(e)
+
     def turn(v, carry):
-        arrive(v)
-        pl.when(jnp.logical_or(v % cuts == 0, v == special))(lambda: down_ready(v // cuts))
-        compute(v)
+        pl.when(jnp.logical_not(lands))(lambda: pass_on(v))
+
+        @pl.when(v >= special + lag)
+        def _():
+            w = v - lag
+            arrive(w)
+            pl.when(jnp.logical_or(w % cuts == 0, w == special))(lambda: down_ready(w // cuts))
+            compute(w)
+
         return carry
 
-    lax.fori_loop(special, blocks - 1, turn, 0)
+    lag = 2
+    lax.fori_loop(special, blocks, turn, 0)
 
     @pl.when(jnp.logical_and(lands, close))
     def _():
@@ -362,6 +399,10 @@
             hand(1, v).wait_recv()
 
         compute(v)
+    arrive(blocks - 2)
+    if (blocks - 2) % cuts == 0 or blocks - 2 == special:
+        down_ready((blocks - 2) // cuts)
+    compute(blocks - 2)
     if (blocks - 1) // cuts != (blocks - 2) // cuts:
         down_ready(experts - 1)
     ends = list(range(special // 2, special)) + [blocks - 1]
@@ -396,8 +437,15 @@
     span = count // tiles
     column = width // 2
 
+    paired = held == 1 and tiles == 4
+
+    def flip(value, mask):
+        ones, twos = value % 2, value // 2
+        low_bit = ones + mask % 2 - 2 * ones * (mask % 2)
+        return low_bit + 2 * (twos + mask // 2 - 2 * twos * (mask // 2))
+
     def tile_of(k):
-        return lax.rem(high // held + k, tiles)
+        return flip(high, tiles - k) if paired else lax.rem(high // held + k, tiles)
 
     def low_copy(k, c):
         t = tile_of(k)
@@ -414,6 +462,28 @@
             mid.at[to, :, over], high_in.at[shift, :, over],
             high_send.at[shift, c], high_recv.at[shift, c], to * 2 + low, tp,
         )
+
+    def pair_copy(k, c):
+        over = pl.ds(c * column, column)
+        to = flip(high, 2 if k == 2 else 1)
+        return remote(
+            mid.at[tile_of(k), :, over], high_in.at[k, :, over],
+            high_send.at[k, c], high_recv.at[k, c], to * 2 + low, tp,
+        )
+
+    def pair_merge(k):
+        t = tile_of(k)
+        for c in range(2):
+            over = pl.ds(c * column, column)
+            low_copy(k, c).wait_recv()
+            sums = part[t, low, :, over].astype(jnp.float32) + low_in[t, :, over].astype(
+                jnp.float32
+            )
+            if k == 2:
+                pair_copy(1, c).wait_recv()
+                sums = sums + high_in[1, :, over].astype(jnp.float32)
+            mid[t, :, over] = sums.astype(mid.dtype)
+            pair_copy(k, c).start()
 
     def merge(k):
         t = tile_of(k)
@@ -443,25 +513,32 @@
                 part[t * held + n, side_of] = values[start : start + owned].astype(part.dtype)
         for c in range(2):
             low_copy(k, c).start()
-        pl.when(k >= 2)(lambda: merge(k - 1))
+        if paired:
+            for step in range(1, tiles):
+                pl.when(k == step + 1)(functools.partial(pair_merge, step))
+        else:
+            pl.when(k >= 2)(lambda: merge(k - 1))
         return carry
 
     lax.fori_loop(1, tiles + 1, closing, 0)
-    merge(tiles)
+    if not paired:
+        merge(tiles)
     for c in range(2):
         over = pl.ds(c * column, column)
+        if paired:
+            low_copy(tiles, c).wait_recv()
         gathered = part[high, low, :, over].astype(jnp.float32) + low_in[high, :, over].astype(
             jnp.float32
         )
-        for shift in range(1, highs):
-            high_copy(shift, c).wait_recv()
+        for shift in (2, 3) if paired else range(1, highs):
+            (pair_copy if paired else high_copy)(shift, c).wait_recv()
             gathered = gathered + high_in[shift, :, over].astype(jnp.float32)
         mixed[:, over] = gathered.astype(mixed.dtype)
     for c in range(2):
-        for k in range(tiles):
+        for k in range(1, tiles + 1):
             low_copy(k, c).wait_send()
         for shift in range(1, highs):
-            high_copy(shift, c).wait_send()
+            (pair_copy if paired else high_copy)(shift, c).wait_send()
 
     @pl.when(lands)
     def _():
@@ -486,7 +563,7 @@
 
                 only(apart, (a, v) in moved, functools.partial(gone, 0))
                 if (a, v) == split:
-                    pl.when(close)(functools.partial(gone, depth // 2))
+                    pl.when(close)(functools.partial(gone, moving))
             for e in range(experts):
                 down_pass(s, e).wait_send()
 
@@ -546,7 +623,7 @@
     outward.wait()
 
 
-def shards(fs_size, tokens, norm_gain, gate_weight, up_weight, down_weight, routes, route_logit):
+def shards(fs_size, tp_size, tokens, norm_gain, gate_weight, up_weight, down_weight, routes, route_logit):
     experts, depth, width = gate_weight.shape
     _, units, col = down_weight.shape
     rows, features = tokens.shape
@@ -566,7 +643,7 @@
     last = special - special // 2 + 1
     mixed_shape = jax.ShapeDtypeStruct((owned, features), half)
     gate_all, up_all, down_all, _, summed = pl.pallas_call(
-        functools.partial(spread, cuts, special),
+        functools.partial(spread, cuts, special, fs_size, tp_size),
         out_shape=(
             gate_shape, gate_shape, down_shape,
             jax.ShapeDtypeStruct((2, 2, blocks, depth, both), half),
@@ -599,7 +676,7 @@
         + [dma((tiles, 2))] * 2
         + [dma((highs, 2))] * 2,
         compiler_params=pltpu.CompilerParams(
-            has_side_effects=True, vmem_limit_bytes=VMEM_LIMIT
+            has_side_effects=True, vmem_limit_bytes=VMEM_LIMIT, collective_id=0
         ),
         name="spread",
     )(norm_gain[None, :], tokens, routes.T, route_logit.T, gate_weight, up_weight, down_weight)
@@ -623,7 +700,7 @@
 
 def solution(mesh):
     return jax.shard_map(
-        functools.partial(shards, mesh.shape["fs"]),
+        functools.partial(shards, mesh.shape["fs"], mesh.shape["tp"]),
         mesh=mesh,
         in_specs=(
             P("tp", None),

time: 411 us -> 405 us (0.985)
  no operation moved by 1% of the time
where the time goes in v3:
time: 405 us
  Pallas kernels  404 us (100%)
    pallas_call x1, Pallas kernels, shards(): pl.pallas_call(functools.partial(spread, cuts, special, fs_size, tp_size)...  371 us
    pallas_call x1, Pallas kernels, shards(): pl.pallas_call(finish, out_shape=(gate_shape, gate_shape, down_shape, mix...  33.3 us

profile of v3, /device:TPU:0, one launch (start us, length us, event | category | flops | bytes accessed | tf_op | source)
XLA Modules:
  0.0 404.6 jit_solution(15875584592427722194)
XLA Ops:
  0.6 370.6 %spread.1 = (bf16[4,2048,1024]{2,1,0:T(8,128)(2,1)}, bf16[4,2048,1024]{2,1,0:T(8,128)(2,1)}, bf16[4,1024,2048]{2,1,0:T(8,128)(2,1)}, bf16[2,2,8,256,1024]{4,3,2,1,0:T(8,128)(2,1)}, bf16[96,2048]{1,0:T(8,128)(2,1)}) custom-call(f32[1,256]{1,0:T(1,128)} %bitcast.5, bf16[768,2048]{1,0:T(8,128)(2,1)} %tokens.1, s32[2,768]{1,0:T(2,128)} %bitcast.3, ...), custom_call_target="tpu_custom_call" | custom-call | tf_op jit(solution)/shard_map/spread/pallas_call | solution.py:645
  371.3 33.3 %finish.1 = (bf16[4,2048,1024]{2,1,0:T(8,128)(2,1)}, bf16[4,2048,1024]{2,1,0:T(8,128)(2,1)}, bf16[4,1024,2048]{2,1,0:T(8,128)(2,1)}, bf16[96,2048]{1,0:T(8,128)(2,1)}) custom-call(bf16[4,2048,1024]{2,1,0:T(8,128)(2,1)} %get-tuple-element.8.gate_in, bf16[4,2048,1024]{2,1,0:T(8,128)(2,1)} %get-tuple-element.9.up_in, ...), custom_call_target="tpu_custom_call" | custom-call | tf_op jit(solution)/shard_map/finish/pallas_call | solution.py:685

commit v4 on v3

--- a/solution.py
+++ b/solution.py
@@ -410,21 +410,21 @@
         bring_down(v, i).start()
     coming = [p for p in lead[special // 2 * 2 :] + [final]]
 
-    @pl.when(jnp.logical_and(lands, apart))
-    def _():
-        take_all(moved, False)
-
     @pl.when(lands)
     def _():
-        take_all([final], False)
+        for a, v in coming:
+            if (a, v) in moved:
+                pl.when(apart)(functools.partial(take, a, v, False))
+            if (a, v) == final:
+                take(a, v, False)
+            bring(a, v, ends.index(v)).start()
 
     @pl.when(jnp.logical_not(lands))
     def _():
         for a, v in coming:
             hand(a, v).wait_recv()
-
-    for a, v in coming:
-        bring(a, v, ends.index(v)).start()
+            bring(a, v, ends.index(v)).start()
+
     for i, v in enumerate(ends):
         bring_down(v, i).wait()
         bring(0, v, i).wait()

time: 405 us -> 402 us (level)
  no operation moved by 1% of the time
where the time goes in v4:
time: 402 us; the launch traced here: 401 us
  Pallas kernels  400 us (100%)
    pallas_call x1, Pallas kernels, shards(): pl.pallas_call(functools.partial(spread, cuts, special, fs_size, tp_size)...  367 us
    pallas_call x1, Pallas kernels, shards(): pl.pallas_call(finish, out_shape=(gate_shape, gate_shape, down_shape, mix...  33.3 us

profile of v4, /device:TPU:0, one launch (start us, length us, event | category | flops | bytes accessed | tf_op | source)
XLA Modules:
  0.0 401.2 jit_solution(7848415395805165588)
XLA Ops:
  0.6 367.1 %spread.1 = (bf16[4,2048,1024]{2,1,0:T(8,128)(2,1)}, bf16[4,2048,1024]{2,1,0:T(8,128)(2,1)}, bf16[4,1024,2048]{2,1,0:T(8,128)(2,1)}, bf16[2,2,8,256,1024]{4,3,2,1,0:T(8,128)(2,1)}, bf16[96,2048]{1,0:T(8,128)(2,1)}) custom-call(f32[1,256]{1,0:T(1,128)} %bitcast.5, bf16[768,2048]{1,0:T(8,128)(2,1)} %tokens.1, s32[2,768]{1,0:T(2,128)} %bitcast.3, ...), custom_call_target="tpu_custom_call" | custom-call | tf_op jit(solution)/shard_map/spread/pallas_call | solution.py:645
  367.8 33.3 %finish.1 = (bf16[4,2048,1024]{2,1,0:T(8,128)(2,1)}, bf16[4,2048,1024]{2,1,0:T(8,128)(2,1)}, bf16[4,1024,2048]{2,1,0:T(8,128)(2,1)}, bf16[96,2048]{1,0:T(8,128)(2,1)}) custom-call(bf16[4,2048,1024]{2,1,0:T(8,128)(2,1)} %get-tuple-element.8.gate_in, bf16[4,2048,1024]{2,1,0:T(8,128)(2,1)} %get-tuple-element.9.up_in, ...), custom_call_target="tpu_custom_call" | custom-call | tf_op jit(solution)/shard_map/finish/pallas_call | solution.py:685
